TPU v7x, 512 devices: a whole 4x8x8 slice. The times are simulated.
512 devices in a mesh: fs: 64 (over z, y), tp: 8 (over x, core).
Axes of the slice: x: 4, y: 8, z: 8, core: 2. Of those that a mesh axis runs over, the one named last changes fastest.
Arguments:
- tokens: bfloat16 [65536, 2048], P(('fs', 'tp')), may hold values from -8 to 8
- pre_mix_gain: float32 [2048], replicated, may hold values from 0.1 to 1.9
- post_mix_gain: float32 [2048], replicated, may hold values from 0.1 to 1.9
- pre_ffn_gain: float32 [2048], replicated, may hold values from 0.1 to 1.9
- post_ffn_gain: float32 [2048], replicated, may hold values from 0.1 to 1.9
- w_branch: bfloat16 [2048, 1024], P('fs', 'tp'), may hold values from -0.125 to 0.125
- w_gelu: bfloat16 [2048, 1024], P('fs', 'tp'), may hold values from -0.125 to 0.125
- conv_weight: bfloat16 [4, 1024], P(None, 'tp'), may hold values from -3 to 3
- w_rec: bfloat16 [2, 8, 128, 128], P(None, 'tp'), may hold values from -0.5 to 0.5
- w_inp: bfloat16 [2, 8, 128, 128], P(None, 'tp'), may hold values from -0.5 to 0.5
- decay: float32 [2, 1024], P(None, 'tp'), may hold values from 3 to 10
- out_weight_t: bfloat16 [2048, 1024], P('fs', 'tp'), may hold values from -0.1875 to 0.1875
- w_gate: bfloat16 [2048, 3072], P('fs', 'tp'), may hold values from -0.125 to 0.125
- w_up: bfloat16 [2048, 3072], P('fs', 'tp'), may hold values from -0.125 to 0.125
- down_weight_t: bfloat16 [2048, 3072], P('fs', 'tp'), may hold values from -0.109375 to 0.109375
Outputs:
- layer_out: bfloat16 [65536, 2048], P(('fs', 'tp'))
All inputs are finite; a program needn't handle non-finite values.
Results may differ from a plain program's by a relative error of at most 0.014.
Values may be sent and summed in bfloat16 or wider, within the bound.
A program may use at most 64 MiB of HBM per device.

v0:
```python
import jax
import jax.numpy as jnp
from jax import lax
from jax.sharding import PartitionSpec as P

EPS = 1e-06


def in_one_piece(arrays, axis, dim, along):
    both = jnp.concatenate(arrays, axis=along)
    whole, at, finished = (lax.all_gather(both, axis, axis=dim, tiled=True), 0, [])
    for a in arrays:
        finished.append(lax.slice_in_dim(whole, at, at + a.shape[along], axis=along))
        at += a.shape[along]
    return tuple(finished)


def normed(values, gain):
    factor = lax.rsqrt(jnp.mean(values * values, axis=-1, keepdims=True) + EPS)
    return values * factor * gain


def conv_short(branch, conv_weight):
    length = branch.shape[0]
    padded = jnp.pad(branch.astype(jnp.float32), ((2, 1), (0, 0)))
    weights = conv_weight.astype(jnp.float32)
    summed = weights[0] * padded[0:length]
    for offset in range(1, 4):
        summed = summed + weights[offset] * padded[offset : offset + length]
    return summed.astype(jnp.bfloat16)


def combine(earlier, later):
    return (earlier[0] * later[0], later[0] * earlier[1] + later[1])


def recurrence(conv_out, w_rec, w_inp, decay):
    length, channels = conv_out.shape
    blocks = w_rec.shape[0]
    grouped = conv_out.reshape(length, blocks, channels // blocks)
    rate_gate = jax.nn.sigmoid(
        jnp.einsum("lnc,ncd->lnd", grouped, w_rec, preferred_element_type=jnp.float32).reshape(
            length, channels
        )
    )
    inflow = jax.nn.sigmoid(
        jnp.einsum("lnc,ncd->lnd", grouped, w_inp, preferred_element_type=jnp.float32).reshape(
            length, channels
        )
    )
    log_retain = -8.0 * rate_gate * jax.nn.softplus(-decay)
    retain = jnp.exp(log_retain)
    feed = jnp.sqrt(-jnp.expm1(2.0 * log_retain)) * inflow * conv_out.astype(jnp.float32)
    unused_decay, states = lax.associative_scan(combine, (retain, feed), axis=0)
    return states


def gathered_product(normed_rows, left_weight, right_weight):
    row_piece = lax.all_gather(normed_rows, "tp", axis=0, tiled=True)
    return jnp.concatenate(
        [
            jnp.dot(row_piece, left_weight, preferred_element_type=jnp.float32),
            jnp.dot(row_piece, right_weight, preferred_element_type=jnp.float32),
        ],
        axis=1,
    )


def summed_rows(hidden, weight_t):
    return lax.psum_scatter(
        lax.dot_general(
            hidden, weight_t, (((1,), (1,)), ((), ())), preferred_element_type=jnp.float32
        ).astype(jnp.bfloat16),
        "tp",
        scatter_dimension=0,
        tiled=True,
    ).astype(jnp.float32)


def per_device(
    tokens,
    pre_mix_gain,
    post_mix_gain,
    pre_ffn_gain,
    post_ffn_gain,
    w_branch,
    w_gelu,
    conv_weight,
    w_rec,
    w_inp,
    decay,
    out_weight_t,
    w_gate,
    w_up,
    down_weight_t,
):
    branch_all, gelu_all, out_rows = in_one_piece((w_branch, w_gelu, out_weight_t), "fs", 0, 1)
    out_whole = lax.all_gather(out_rows, "tp", axis=1, tiled=True)
    stream = tokens.astype(jnp.float32)
    normed_in = normed(stream, pre_mix_gain).astype(jnp.bfloat16)
    both_in = gathered_product(normed_in, branch_all, gelu_all)
    channels = branch_all.shape[1]
    branch_in = both_in[:, :channels].astype(jnp.bfloat16)
    gelu_in = both_in[:, channels:].astype(jnp.bfloat16)
    conv_out = conv_short(branch_in, conv_weight)
    forward = recurrence(conv_out, w_rec[0], w_inp[0], decay[0])
    backward = jnp.flip(recurrence(jnp.flip(conv_out, 0), w_rec[1], w_inp[1], decay[1]), 0)
    mixer_hidden = (jax.nn.gelu(gelu_in.astype(jnp.float32)) * (forward + backward)).astype(
        jnp.bfloat16
    )
    own_hidden = lax.all_to_all(mixer_hidden, "tp", split_axis=0, concat_axis=1, tiled=True)
    mixer_sum = lax.dot_general(
        own_hidden, out_whole, (((1,), (1,)), ((), ())), preferred_element_type=jnp.float32
    )
    residual = (stream + normed(mixer_sum, post_mix_gain)).astype(jnp.bfloat16)
    middle = residual.astype(jnp.float32)
    normed_mid = normed(middle, pre_ffn_gain).astype(jnp.bfloat16)
    gate_all, up_all, down_all = in_one_piece((w_gate, w_up, down_weight_t), "fs", 0, 1)
    both_mid = gathered_product(normed_mid, gate_all, up_all)
    hidden_units = gate_all.shape[1]
    gate_proj = both_mid[:, :hidden_units]
    up_proj = both_mid[:, hidden_units:]
    ffn_hidden = (jax.nn.silu(gate_proj) * up_proj).astype(jnp.bfloat16)
    ffn_sum = summed_rows(ffn_hidden, down_all)
    return (middle + normed(ffn_sum, post_ffn_gain)).astype(jnp.bfloat16)


def solution(mesh):
    return jax.shard_map(
        per_device,
        mesh=mesh,
        in_specs=(
            P(("fs", "tp"), None),
            P(),
            P(),
            P(),
            P(),
            P("fs", "tp"),
            P("fs", "tp"),
            P(None, "tp"),
            P(None, "tp", None, None),
            P(None, "tp", None, None),
            P(None, "tp"),
            P("fs", "tp"),
            P("fs", "tp"),
            P("fs", "tp"),
            P("fs", "tp"),
        ),
        out_specs=P(("fs", "tp"), None),
        check_vma=False,
    )
```

profile of v0, /device:TPU:1, one launch (start us, length us, event | category | flops | bytes accessed | tf_op | source)
XLA Modules:
  0.0 371.8 jit_solution(1877080650165406262)
XLA Ops:
  6.5 1.3 pad_maximum_fusion.9
  7.9 1.2 fusion.29
  9.2 2.0 fusion.31
  11.3 82.9 %all-gather.8.cloned.1.call-done = bf16[2048,384]{1,0:T(8,128)(2,1)} async-done(((bf16[32,384]{1,0:T(8,128)(2,1)}), bf16[2048,384]{1,0:T(8,128)(2,1)}) %all-gather.8.cloned.1.call-update) | async-done | bytes 1572880 | tf_op jit(solution)/shard_map/all_gather | solution.py:11
  94.2 1.9 slice.729
  96.1 1.4 pad_maximum_fusion.4
  98.3 0.8 fusion.75
  99.1 36.5 %all-gather.6.cloned.1.call-done = bf16[1024,2048]{1,0:T(8,128)(2,1)} async-done(((bf16[128,2048]{1,0:T(8,128)(2,1)}), bf16[1024,2048]{1,0:T(8,128)(2,1)}) %all-gather.6.cloned.1.call-update) | async-done | bytes 4194320 | tf_op jit(solution)/shard_map/all_gather | solution.py:59
  135.6 3.5 fusion.25
  181.9 0.8 fusion.59
  184.9 1.7 pad.146
  186.7 1.7 pad.145
  188.4 0.8 fusion.94
  191.1 3.6 fusion.48
  194.9 9.5 %all_to_all.19 = bf16[8,128,128]{1,2,0:T(8,128)(2,1)S(1)} all-to-all(bf16[8,128,128]{1,2,0:T(8,128)(2,1)S(1)} %copy.16), channel_id=1, replica_groups=mesh['fs'=64,'tp'=8] {'tp'}, dimensions={0} | all-to-all | bytes 524288 | tf_op jit(solution)/shard_map/all_to_all | solution.py:111
  204.4 3.8 %multiply_reduce_fusion = (f32[128]{0:T(128)S(1)}, f32[128,2048]{1,0:T(8,128)S(1)}) fusion(bf16[128,1024]{0,1:T(8,128)(2,1)S(1)} %bitcast.42, bf16[2048,1024]{1,0:T(8,128)(2,1)} %all-gather.10.cloned.1.call-done), kind=kOutput, calls=%fused_computation.51 | convolution fusion | flops 537395072 | bytes 5505536 | tf_op jit(solution)/shard_map/dot_general | solution.py:112
  208.6 1.0 fusion.35
  209.8 55.5 %all-gather.14.cloned.1.call-done = bf16[2048,1152]{1,0:T(8,128)(2,1)} async-done(((bf16[32,1152]{1,0:T(8,128)(2,1)}), bf16[2048,1152]{1,0:T(8,128)(2,1)}) %all-gather.14.cloned.1.call-update) | async-done | bytes 4718608 | tf_op jit(solution)/shard_map/all_gather | solution.py:11
  265.3 40.5 %all-gather.12.cloned.1.call-done = bf16[1024,2048]{1,0:T(8,128)(2,1)} async-done(((bf16[128,2048]{1,0:T(8,128)(2,1)}), bf16[1024,2048]{1,0:T(8,128)(2,1)}) %all-gather.12.cloned.1.call-update) | async-done | bytes 4194320 | tf_op jit(solution)/shard_map/all_gather | solution.py:59
  305.8 5.0 %fusion.3 = f32[1024,384]{1,0:T(8,128)S(1)} fusion(bf16[1024,2048]{1,0:T(8,128)(2,1)} %all-gather.12.cloned.1.call-done, bf16[2048,1152]{1,0:T(8,128)(2,1)} %all-gather.14.cloned.1.call-done), kind=kOutput, calls=%fused_computation.4 | convolution fusion | flops 1610612736 | bytes 7340032 | tf_op jit(solution)/shard_map/dot_general | solution.py:62
  310.8 9.7 %convolution_convert_fusion = bf16[1024,2048]{1,0:T(8,128)(2,1)} fusion(bf16[2048,1152]{1,0:T(8,128)(2,1)} %all-gather.14.cloned.1.call-done, f32[1024,384]{1,0:T(8,128)S(1)} %fusion.3, bf16[1024,2048]{1,0:T(8,128)(2,1)} %all-gather.12.cloned.1.call-done), kind=kOutput, calls=%fused_computation | convolution fusion | flops 3225681920 | bytes 13107200 | tf_op jit(solution)/shard_map/dot_general | solution.py:71
  320.5 41.1 %reduce-scatter.2.cloned.1.call-done = bf16[128,2048]{1,0:T(8,128)(2,1)} async-done(((bf16[1024,2048]{1,0:T(8,128)(2,1)}), bf16[128,2048]{1,0:T(8,128)(2,1)}) %reduce-scatter.2.cloned.1.call-update) | async-done | bytes 524304 | tf_op jit(solution)/shard_map/reduce_scatter | solution.py:70
  361.6 1.2 fusion.27
  362.8 2.1 fusion.36
  (331 shorter events, 47.4 us)
Async XLA Ops:
  6.5 87.6 %all-gather.8.cloned.1.call-start = ((), (), s32[]{:S(2)}) async-start(), calls=%async_computation.3 | async-start | bytes 1597440 | tf_op jit(solution)/shard_map/all_gather | solution.py:11
  7.9 127.7 %all-gather.6.cloned.1.call-start = ((), (), s32[]{:S(2)}) async-start(), calls=%async_computation.2 | async-start | bytes 4718592 | tf_op jit(solution)/shard_map/all_gather | solution.py:59
  11.2 193.2 %all-gather.10.cloned.1.call-start = ((), (), s32[]{:S(2)}) async-start(), calls=%async_computation.4 | async-start | bytes 4718592 | tf_op jit(solution)/shard_map/all_gather | solution.py:98
  96.0 43.3 %copy-start.35 = (bf16[2,1,128,128]{3,2,1,0:T(8,128)(2,1)S(1)}, bf16[2,1,128,128]{3,2,1,0:T(8,128)(2,1)}, u32[]{:S(2)}) copy-start(bf16[2,1,128,128]{3,2,1,0:T(8,128)(2,1)} %param.23) | copy-start | bytes 196612
  96.1 169.2 %all-gather.14.cloned.1.call-start = ((), (), s32[]{:S(2)}) async-start(), calls=%async_computation.6 | async-start | bytes 4792320 | tf_op jit(solution)/shard_map/all_gather | solution.py:11
  97.5 208.2 %all-gather.12.cloned.1.call-start = ((), (), s32[]{:S(2)}) async-start(), calls=%async_computation.5 | async-start | bytes 4718592 | tf_op jit(solution)/shard_map/all_gather | solution.py:59
  99.1 40.7 %copy-start.36 = (bf16[2,1,128,128]{3,2,1,0:T(8,128)(2,1)S(1)}, bf16[2,1,128,128]{3,2,1,0:T(8,128)(2,1)}, u32[]{:S(2)}) copy-start(bf16[2,1,128,128]{3,2,1,0:T(8,128)(2,1)} %param.24) | copy-start | bytes 196612
  140.3 15.6 %copy-start.2 = (f32[1024,128]{1,0:T(8,128)}, f32[1024,128]{1,0:T(8,128)S(1)}, u32[]{:S(2)}) copy-start(f32[1024,128]{1,0:T(8,128)S(1)} %fusion.21) | copy-start | bytes 1572868
  157.1 17.5 %copy-start.1 = (f32[1024,128]{1,0:T(8,128)}, f32[1024,128]{1,0:T(8,128)S(1)}, u32[]{:S(2)}) copy-start(f32[1024,128]{1,0:T(8,128)S(1)} %fusion.24) | copy-start | bytes 1572868
  159.7 26.9 %copy-start.16 = (f32[4,128]{1,0:T(4,128)}, f32[4,128]{1,0:T(4,128)S(1)}, u32[]{:S(2)}) copy-start(f32[4,128]{1,0:T(4,128)S(1)} %get-tuple-element.42) | copy-start | bytes 6148
  159.7 26.9 %copy-start.18 = (f32[4,128]{1,0:T(4,128)}, f32[4,128]{1,0:T(4,128)S(1)}, u32[]{:S(2)}) copy-start(f32[4,128]{1,0:T(4,128)S(1)} %get-tuple-element.41) | copy-start | bytes 6148
  172.9 13.7 %slice-start.1 = ((f32[1024,128]{1,0:T(8,128)}), f32[1,128]{1,0:T(1,128)S(1)}, s32[]{:S(2)}) async-start(f32[1024,128]{1,0:T(8,128)} %copy-done.2), calls=%async_computation.9 | async-start | bytes 1024 | tf_op jit(solution)/shard_map/slice | solution.py:54
  175.3 13.1 %copy-start.24 = (f32[2,128]{1,0:T(2,128)S(1)}, f32[2,128]{1,0:T(2,128)}, u32[]{:S(2)}) copy-start(f32[2,128]{1,0:T(2,128)} %slice.661) | copy-start | bytes 3076
  175.3 13.1 %copy-start.25 = (f32[2,128]{1,0:T(2,128)S(1)}, f32[2,128]{1,0:T(2,128)}, u32[]{:S(2)}) copy-start(f32[2,128]{1,0:T(2,128)} %slice.662) | copy-start | bytes 3076
  175.3 13.1 %copy-start.26 = (f32[2,128]{1,0:T(2,128)S(1)}, f32[2,128]{1,0:T(2,128)}, u32[]{:S(2)}) copy-start(f32[2,128]{1,0:T(2,128)} %slice.660) | copy-start | bytes 3076
  175.3 13.1 %copy-start.27 = (f32[2,128]{1,0:T(2,128)S(1)}, f32[2,128]{1,0:T(2,128)}, u32[]{:S(2)}) copy-start(f32[2,128]{1,0:T(2,128)} %slice.664) | copy-start | bytes 3076
  176.9 12.4 %copy-start.22 = (f32[3,128]{1,0:T(4,128)S(1)}, f32[3,128]{1,0:T(4,128)}, u32[]{:S(2)}) copy-start(f32[3,128]{1,0:T(4,128)} %slice.653) | copy-start | bytes 4612
  176.9 12.4 %copy-start.23 = (f32[3,128]{1,0:T(4,128)S(1)}, f32[3,128]{1,0:T(4,128)}, u32[]{:S(2)}) copy-start(f32[3,128]{1,0:T(4,128)} %slice.670) | copy-start | bytes 4612
  177.5 11.8 %copy-start.13 = (f32[7,128]{1,0:T(8,128)S(1)}, f32[7,128]{1,0:T(8,128)}, u32[]{:S(2)}) copy-start(f32[7,128]{1,0:T(8,128)} %slice.647) | copy-start | bytes 10756
  194.7 13.5 %copy-start = (bf16[128,2048]{1,0:T(8,128)(2,1)S(1)}, bf16[128,2048]{1,0:T(8,128)(2,1)}, u32[]{:S(2)}) copy-start(bf16[128,2048]{1,0:T(8,128)(2,1)} %param.15) | copy-start | bytes 1572868
  194.7 13.5 %copy-start.19 = (f32[2048]{0:T(1024)S(1)}, f32[2048]{0:T(1024)}, u32[]{:S(2)}) copy-start(f32[2048]{0:T(1024)} %param.17) | copy-start | bytes 24580
  194.9 13.7 %copy-start.20 = (f32[2048]{0:T(1024)S(1)}, f32[2048]{0:T(1024)}, u32[]{:S(2)}) copy-start(f32[2048]{0:T(1024)} %param.18) | copy-start | bytes 24580
  209.6 152.0 %reduce-scatter.2.cloned.1.call-start = ((), (), s32[]{:S(2)}) async-start(), calls=%async_computation.7 | async-start | bytes 4718592 | tf_op jit(solution)/shard_map/reduce_scatter | solution.py:70
  320.5 42.3 %copy-start.21 = (f32[2048]{0:T(1024)S(1)}, f32[2048]{0:T(1024)}, u32[]{:S(2)}) copy-start(f32[2048]{0:T(1024)} %param.19) | copy-start | bytes 24580
  (21 other events, 168.1 us)
Sparse Core Ops, SparseCore 0:
  10.3 83.7 all-gather.7
  96.3 39.2 all-gather.5
  137.7 40.8 all-gather.9
  181.5 83.7 all-gather.13
  267.3 38.4 all-gather.11
  320.6 40.9 reduce-scatter.1
where the time goes:
time: 374 us; the launch traced here: 372 us
  waiting for transfers between devices  257 us (69%)
  local copies, waits for them, and re-layouts  39.3 us (11%)
  matrix products  27.3 us (7%)
  other arithmetic  23.8 us (6%)
  between operations  15 us (4%)
  blocking collectives  9.49 us (3%)
    all_gather x2, waiting for transfers between devices, in_one_piece(): lax.all_gather(both, axis, axis=dim, tiled=True)  138 us
    all_gather x2, waiting for transfers between devices, gathered_product(): row_piece = lax.all_gather(normed_rows, 'tp', axis=0, tiled=True)  77 us
    reduce_scatter x1, waiting for transfers between devices, summed_rows(): lax.psum_scatter(lax.dot_general(hidden, weight_t, (((1,), (1,)), ((), ()...  41.1 us
    slice x122, local copies, waits for them, and re-layouts, recurrence(): unused_decay, states = lax.associative_scan(combine, (retain, feed), axis=0)  32.3 us
    dot_general x1, matrix products, summed_rows(): lax.dot_general(hidden, weight_t, (((1,), (1,)), ((), ())), preferred_ele...  9.7 us
    all_to_all x1, blocking collectives, per_device(): lax.all_to_all(mixer_hidden, 'tp', split_axis=0, concat_axis=1, tiled=True)  9.49 us
    dot_general x2, matrix products, gathered_product(): jnp.dot(row_piece, left_weight, preferred_element_type=jnp.float32)  8.53 us
  transfers between devices with their start and end apart: 6, of which 5 were waited for; matrix products, arithmetic and copies ran while one was open for 19% of the time, Pallas kernels for 0%

commit v1 on v0

v1 whole, which is shorter than its diff:
```python
import jax
import jax.numpy as jnp
from jax import lax
from jax.experimental import pallas as pl
from jax.experimental.pallas import tpu as pltpu
from jax.sharding import PartitionSpec as P

EPS = 1e-06
MESH = pl.DeviceIdType.MESH
F32 = jnp.float32
BF16 = jnp.bfloat16
RING = 8
CHIPS = 4
ROWS = 128
SUB = 32
SUBS = ROWS // SUB
D = 2048
SEG = 136
NT = (((1,), (1,)), ((), ()))


def rem(a, n):
    return lax.rem(a, jnp.int32(n))


def hold(ref, sem):
    pltpu.make_async_copy(ref, ref, sem).wait()


def normed(values, gain):
    factor = lax.rsqrt(jnp.mean(values * values, axis=-1, keepdims=True) + EPS)
    return values * factor * gain


def sigmoid(v):
    return 1.0 / (1.0 + jnp.exp(-v))


def gelu(v):
    return 0.5 * v * (1.0 + jnp.tanh(0.7978845608028654 * (v + 0.044715 * v * v * v)))


def loop(count, body):
    def step(i, carry):
        body(i)
        return carry

    lax.fori_loop(0, count, step, 0)


def layer(
    tokens,
    pre_mix,
    post_mix,
    pre_ffn,
    post_ffn,
    w_branch,
    w_gelu,
    conv_weight,
    w_rec,
    w_inp,
    decay,
    out_w,
    w_gate,
    w_up,
    w_down,
    out,
    tok,
    n1,
    n2,
    a_all,
    o_all,
    f_all,
    o_own,
    branch,
    gel,
    ret0,
    ret1,
    fee0,
    fee1,
    gates,
    scale,
    carry_in,
    mixed,
    hidden,
    msum,
    res,
    gu,
    hid,
    keep,
    give,
    got,
    sums,
    land,
    load_sem,
    a_recv,
    o_recv,
    f_recv,
    ring_send,
    pre_recv,
    pre_send,
    swap_recv,
    swap_send,
    n1_recv,
    n2_recv,
    n_send,
    mix_recv,
    mix_send,
    pair_recv,
    pair_send,
    land_recv,
    land_send,
):
    f = lax.axis_index("fs")
    t = lax.axis_index("tp")
    z, y = lax.div(f, jnp.int32(RING)), rem(f, RING)
    x, c = lax.div(t, jnp.int32(2)), rem(t, 2)
    p, q = y + c * (z - y), z + c * (y - z)
    step_p, step_q = 1 + (RING - 1) * c, RING - (RING - 1) * c
    turn = 1 - 2 * c
    partner = 2 * x + 1 - c

    def place(pp, qq):
        return pp * step_p + qq * step_q

    def remote(src, dst, send, recv, fs=None, tp=None):
        return pltpu.make_async_remote_copy(
            src_ref=src,
            dst_ref=dst,
            send_sem=send,
            recv_sem=recv,
            device_id={"fs": f if fs is None else fs, "tp": t if tp is None else tp},
            device_id_type=MESH,
        )

    def chip(away):
        return rem(x + away + CHIPS, CHIPS)

    loads = [
        (w_branch, a_all.at[f, :, pl.ds(0, 128)]),
        (w_gelu, a_all.at[f, :, pl.ds(128, 128)]),
        (out_w, o_own),
        (tokens, tok),
        (w_gate, f_all.at[f, :, pl.ds(0, 384)]),
        (w_up, f_all.at[f, :, pl.ds(384, 384)]),
        (w_down, f_all.at[f, :, pl.ds(768, 384)]),
    ]
    loads = [pltpu.make_async_copy(s, d, load_sem.at[i]) for i, (s, d) in enumerate(loads)]
    for copy in loads:
        copy.start()

    barrier = pltpu.get_barrier_semaphore()

    def greet(fs, tp):
        pl.semaphore_signal(barrier, inc=1, device_id={"fs": fs, "tp": tp}, device_id_type=MESH)

    for e in range(1, RING):
        greet(place(rem(p + e, RING), q), t)
    for e in (1, RING - 1):
        greet(place(p, rem(q + e, RING)), t)
    for e in range(1, 8):
        greet(f, rem(t + e, 8))
    pl.semaphore_wait(barrier, 16)

    class Gather:
        def __init__(self, piece, recv, send):
            self.piece, self.recv, self.send = piece, recv, send

        def spread(self):
            def body(e):
                j = e + 1
                off = lax.div(j + 1, jnp.int32(2)) * (2 * rem(j, 2) - 1)
                there = place(rem(p + off + RING, RING), q)
                remote(self.piece(f), self.piece(f), self.send, self.recv.at[f], fs=there).start()

            loop(RING - 1, body)

        def slot(self, j, away):
            off = lax.div(j + 1, jnp.int32(2)) * (2 * rem(j, 2) - 1)
            return place(rem(p + off + RING, RING), rem(q + away + RING, RING))

        def pass_on(self, slot, way):
            there = place(p, rem(q + way + RING, RING))
            remote(
                self.piece(slot), self.piece(slot), self.send, self.recv.at[slot], fs=there
            ).start()

        def arrive(self, slot):
            hold(self.piece(slot), self.recv.at[slot])

        def first(self, half):
            def body(i):
                j = i + 4 * half
                slot = self.slot(j, 0)

                @pl.when(j > 0)
                def _():
                    self.arrive(slot)

                self.pass_on(slot, 1)
                self.pass_on(slot, -1)

            loop(4, body)

        def hop(self, far, half):
            def body(i):
                j = i + 4 * half
                k = j + 4 if far == 3 else j
                from_left, from_right = self.slot(j, -far), self.slot(k, far)
                self.arrive(from_left)
                self.pass_on(from_left, 1)
                self.arrive(from_right)
                self.pass_on(from_right, -1)

            loop(4, body)

        def finish(self):
            def body(j):
                self.arrive(self.slot(j + 4, -3))
                self.arrive(self.slot(j, 3))
                self.arrive(self.slot(j, 4))
                self.arrive(self.slot(j + 4, 4))

            loop(4, body)

    ga = Gather(lambda s: a_all.at[s], a_recv, ring_send.at[0])
    go = Gather(lambda s: o_all.at[s, c], o_recv, ring_send.at[1])
    gf = Gather(lambda s: f_all.at[s], f_recv, ring_send.at[2])

    loads[0].wait()
    loads[1].wait()
    ga.spread()

    loads[2].wait()
    own_lanes = pl.ds(pl.multiple_of(t * 128, 128), 128)
    for e in range(1, 8):
        other = rem(t + e, 8)
        half = rem(other, 2)
        remote(
            o_own.at[half], o_all.at[f, half, :, own_lanes], pre_send, pre_recv.at[t], tp=other
        ).start()
    own_out = pltpu.make_async_copy(o_own.at[c], o_all.at[f, c, :, own_lanes], load_sem.at[7])
    own_out.start()

    class Rows:
        def __init__(self, ref, recv, send):
            self.ref, self.recv, self.send = ref, recv, send

        def pass_on(self, at, tp):
            remote(self.ref.at[at], self.ref.at[at], self.send, self.recv.at[at], tp=tp).start()

        def arrive(self, at):
            hold(self.ref.at[at], self.recv.at[at])

        def own(self, k):
            at = t * SUBS + k
            self.pass_on(at, 2 * chip(turn) + c)
            self.pass_on(at, 2 * chip(-turn) + c)
            self.pass_on(at, partner)

        def behind(self, k):
            at = (2 * chip(-turn) + c) * SUBS + k
            self.arrive(at)
            self.pass_on(at, 2 * chip(turn) + c)
            self.pass_on(at, partner)

        def ahead(self, k):
            at = (2 * chip(turn) + c) * SUBS + k
            self.arrive(at)
            self.pass_on(at, partner)

        def far(self, k):
            at = (2 * chip(2) + c) * SUBS + k
            self.arrive(at)
            self.pass_on(at, partner)

        def paired(self, chip_at):
            for k in range(SUBS):
                self.arrive((2 * chip_at + 1 - c) * SUBS + k)

        def drain(self):
            hold(self.ref.at[pl.ds(0, 7 * SUBS)], self.send)

        def block(self, tp):
            rows = self.ref[pl.ds(tp * SUBS, SUBS)]
            return rows.reshape(ROWS, D)

    r1 = Rows(n1, n1_recv, n_send.at[0])
    r2 = Rows(n2, n2_recv, n_send.at[1])

    loads[3].wait()

    def norm_in(k):
        for h in range(SUB // 16):
            rows = tok[pl.ds(pl.multiple_of(k * SUB + 16 * h, 16), 16), :].astype(F32)
            n1[t * SUBS + k, pl.ds(16 * h, 16), :] = normed(rows, pre_mix[...]).astype(BF16)
        r1.own(k)

    loop(SUBS, norm_in)

    ga.first(0)
    ga.first(1)
    for d in range(2):
        gates[:, pl.ds(256 * d, 128)] = w_rec[d, 0]
        gates[:, pl.ds(256 * d + 128, 128)] = w_inp[d, 0]
    low = -decay[...]
    scale[...] = -8.0 * (jnp.maximum(low, 0.0) + jnp.log1p(jnp.exp(-jnp.abs(low))))
    branch[pl.ds(0, 8), :] = jnp.zeros((8, 128), F32)
    branch[pl.ds(1032, 8), :] = jnp.zeros((8, 128), F32)

    own_out.wait()
    for e in range(1, 8):
        other = rem(t + e, 8)
        lanes = pl.ds(pl.multiple_of(other * 128, 128), 128)
        hold(o_all.at[f, c, :, lanes], pre_recv.at[other])
    ga.hop(1, 0)
    go.spread()
    ga.hop(1, 1)
    r1.behind(0)
    r1.ahead(0)
    ga.hop(2, 0)
    ga.hop(2, 1)
    r1.behind(1)
    r1.ahead(1)
    go.first(0)
    ga.hop(3, 0)
    go.first(1)
    r1.behind(2)
    r1.ahead(2)
    loads[4].wait()
    loads[5].wait()
    loads[6].wait()
    gf.spread()
    ga.finish()
    r1.behind(3)
    r1.ahead(3)

    def project(chip_at):
        r1.paired(chip_at)
        rows = n1[pl.ds(2 * chip_at * SUBS, 2 * SUBS)].reshape(2 * ROWS, D)
        both = jnp.dot(rows, a_all[...].reshape(D, 256), preferred_element_type=F32)
        both = both.astype(BF16).astype(F32)
        at = chip_at * 2 * ROWS
        branch[pl.ds(pl.multiple_of(at + 8, 8), 2 * ROWS), :] = both[:, :128]
        gel[pl.ds(pl.multiple_of(at, 8), 2 * ROWS), :] = both[:, 128:]

    project(x)
    go.hop(1, 0)
    project(chip(turn))
    go.hop(1, 1)
    project(chip(-turn))
    go.hop(2, 0)
    for k in range(SUBS):
        r1.far(k)
    project(chip(2))

    taps = conv_weight[...].astype(F32)

    def gate(s):
        window = branch[pl.ds(pl.multiple_of(s * 128, 8), 144), :]
        summed = taps[0:1] * window[6:134]
        for offset in range(1, 4):
            summed = summed + taps[offset : offset + 1] * window[6 + offset : 134 + offset]
        conv = summed.astype(BF16)
        wide = conv.astype(F32)
        both = jnp.dot(conv, gates[...], preferred_element_type=F32)
        at = pl.ds(pl.multiple_of(s * SEG, 8), 128)
        for d, (ret, fee) in enumerate(((ret0, fee0), (ret1, fee1))):
            rate = sigmoid(both[:, 256 * d : 256 * d + 128])
            inflow = sigmoid(both[:, 256 * d + 128 : 256 * d + 256])
            log_retain = rate * scale[pl.ds(d, 1), :]
            retain = jnp.exp(log_retain)
            u = 2.0 * log_retain
            near = 1.0 + u * (0.2 * (1.0 + u * (1.0 / 6.0)))
            near = 1.0 + u * (1.0 / 3.0) * (1.0 + u * 0.25 * near)
            near = -u * (1.0 + 0.5 * u * near)
            lost = jnp.where(u > -0.25, near, 1.0 - retain * retain)
            ret[at, :] = retain
            fee[at, :] = jnp.sqrt(lost) * inflow * wide

    loop(8, gate)
    go.hop(2, 1)

    one, zero = jnp.ones((8, 128), F32), jnp.zeros((8, 128), F32)

    def scan(i, carry):
        h0, a0, h1, a1 = carry
        for k in range(8):
            up = pl.ds(i * 8 + k, 8, stride=SEG)
            down = pl.ds(127 - (i * 8 + k), 8, stride=SEG)
            r, v = ret0[up, :], fee0[up, :]
            h0 = r * h0 + v
            a0 = r * a0
            fee0[up, :] = h0
            ret0[up, :] = a0
            r, v = ret1[down, :], fee1[down, :]
            h1 = r * h1 + v
            a1 = r * a1
            fee1[down, :] = h1
            ret1[down, :] = a1
        return h0, a0, h1, a1

    h0, a0, h1, a1 = lax.fori_loop(0, 16, scan, (zero, one, zero, one))
    state = jnp.zeros((1, 128), F32)
    for s in range(8):
        carry_in[s : s + 1, :] = state
        state = a0[s : s + 1] * state + h0[s : s + 1]
    state = jnp.zeros((1, 128), F32)
    for s in reversed(range(8)):
        carry_in[8 + s : 9 + s, :] = state
        state = a1[s : s + 1] * state + h1[s : s + 1]

    def mix(e):
        s = rem(t + e, 8)
        at = pl.ds(pl.multiple_of(s * SEG, 8), 128)
        state = fee0[at, :] + ret0[at, :] * carry_in[pl.ds(s, 1), :]
        state = state + (fee1[at, :] + ret1[at, :] * carry_in[pl.ds(8 + s, 1), :])
        value = gelu(gel[pl.ds(pl.multiple_of(s * 128, 8), 128), :]) * state
        mixed[s] = value.astype(BF16)

        @pl.when(e > 0)
        def _():
            remote(mixed.at[s], hidden.at[t], mix_send, mix_recv.at[t], tp=s).start()

        @pl.when(e == 0)
        def _():
            hidden[s] = value.astype(BF16)

    loop(8, mix)
    go.hop(3, 0)
    gf.first(0)
    gf.first(1)
    go.finish()

    def swap(part):
        rows = o_all.at[pl.ds(16 * part, 16), c]
        remote(rows, rows, swap_send, swap_recv.at[part], tp=partner).start()

    loop(4, swap)
    for e in range(1, 8):
        other = rem(t + e, 8)
        hold(hidden.at[other], mix_recv.at[other])
    gf.hop(1, 0)

    wide_hidden = jnp.concatenate([hidden[i] for i in range(8)], axis=1)

    def project_out(part):
        hold(o_all.at[pl.ds(16 * part, 16), 1 - c], swap_recv.at[part])
        weight = o_all[pl.ds(16 * part, 16)].reshape(512, 1024)
        msum[:, pl.ds(pl.multiple_of(part * 512, 128), 512)] = lax.dot_general(
            wide_hidden, weight, NT, preferred_element_type=F32
        )

    loop(4, project_out)

    def norm_mid(k):
        for h in range(SUB // 16):
            at = pl.ds(pl.multiple_of(k * SUB + 16 * h, 16), 16)
            total = tok[at, :].astype(F32) + normed(msum[at, :], post_mix[...])
            total = total.astype(BF16)
            res[at, :] = total
            n2[t * SUBS + k, pl.ds(16 * h, 16), :] = normed(
                total.astype(F32), pre_ffn[...]
            ).astype(BF16)
        r2.own(k)

    loop(SUBS, norm_mid)
    gf.hop(1, 1)
    gf.hop(2, 0)
    for k in range(SUBS):
        r2.behind(k)
        r2.ahead(k)
    gf.hop(2, 1)
    gf.hop(3, 0)
    for k in range(SUBS):
        r2.far(k)
    gf.finish()

    def feed_forward(i):
        away = jnp.where(i == 0, 2, jnp.where(i == 1, -turn, jnp.where(i == 2, turn, 0)))
        there = chip(away)
        r2.paired(there)
        rows = jnp.concatenate([r2.block(2 * there + 1 - c), r2.block(2 * there + c)], axis=0)
        for n in range(3):
            gu[:, pl.ds(256 * n, 256)] = jnp.dot(
                rows, f_all[:, :, pl.ds(256 * n, 256)].reshape(D, 256), preferred_element_type=F32
            )
        for h in range(4):
            at = pl.ds(64 * h, 64)
            g = gu[at, pl.ds(0, 384)]
            hid[at, :] = (g * sigmoid(g) * gu[at, pl.ds(384, 384)]).astype(BF16)

        def down(n):
            weight = f_all[pl.ds(16 * n, 16), :, pl.ds(768, 384)].reshape(512, 384)
            part = lax.dot_general(hid[...], weight, NT, preferred_element_type=F32)
            lanes = pl.ds(pl.multiple_of(512 * n, 128), 512)
            give[i, :, lanes] = part[:ROWS].astype(BF16)
            keep[i, :, lanes] = part[ROWS:]

        loop(4, down)
        other = jnp.where(i == 1, 2, jnp.where(i == 2, 1, i))
        remote(give.at[i], got.at[other], pair_send, pair_recv.at[other], tp=partner).start()

        @pl.when(i == 1)
        def _():
            pass_sum(0)

    def pass_sum(o):
        target = 2 * chip(-turn if o == 1 else turn) + c
        hold(got.at[o], pair_recv.at[o])

        def add(k):
            if o == 2:
                hold(land.at[0, k], land_recv.at[0, k])
            for h in range(SUB // 16):
                at = pl.ds(pl.multiple_of(k * SUB + 16 * h, 16), 16)
                inner = pl.ds(16 * h, 16)
                total = keep[o, at, :] + got[o, at, :].astype(F32)
                if o == 2:
                    total = total + land[0, k, inner, :].astype(F32)
                sums[o, k, inner, :] = total.astype(BF16)
            remote(
                sums.at[o, k], land.at[o, k], land_send, land_recv.at[o, k], tp=target
            ).start()

        loop(SUBS, add)

    loop(4, feed_forward)
    pass_sum(1)
    pass_sum(2)
    hold(got.at[3], pair_recv.at[3])

    def last(k):
        hold(land.at[1, k], land_recv.at[1, k])
        hold(land.at[2, k], land_recv.at[2, k])
        for h in range(SUB // 16):
            at = pl.ds(pl.multiple_of(k * SUB + 16 * h, 16), 16)
            inner = pl.ds(16 * h, 16)
            total = keep[3, at, :] + got[3, at, :].astype(F32)
            total = total + land[1, k, inner, :].astype(F32)
            total = total + land[2, k, inner, :].astype(F32)
            final = res[at, :].astype(F32) + normed(total, post_ffn[...])
            out[at, :] = final.astype(BF16)

    loop(SUBS, last)

    hold(a_all.at[pl.ds(0, 63)], ring_send.at[0])
    hold(o_all.at[pl.ds(0, 63), 0], ring_send.at[1])
    hold(f_all.at[pl.ds(0, 63)], ring_send.at[2])
    hold(o_all.at[0, 0, :, pl.ds(0, 896)], pre_send)
    hold(o_all.at[:, c], swap_send)
    r1.drain()
    r2.drain()
    hold(mixed.at[pl.ds(0, 7)], mix_send)
    hold(give, pair_send)
    hold(sums, land_send)


def per_device(
    tokens,
    pre_mix_gain,
    post_mix_gain,
    pre_ffn_gain,
    post_ffn_gain,
    w_branch,
    w_gelu,
    conv_weight,
    w_rec,
    w_inp,
    decay,
    out_weight_t,
    w_gate,
    w_up,
    down_weight_t,
):
    gains = [
        g.reshape(1, D) for g in (pre_mix_gain, post_mix_gain, pre_ffn_gain, post_ffn_gain)
    ]
    vmem = pl.BlockSpec(memory_space=pltpu.VMEM)
    far = pl.BlockSpec(memory_space=pl.ANY)
    dma = pltpu.SemaphoreType.DMA
    return pl.pallas_call(
        layer,
        out_shape=jax.ShapeDtypeStruct((ROWS, D), BF16),
        in_specs=[far] + [vmem] * 4 + [far, far] + [vmem] * 4 + [far] * 4,
        out_specs=vmem,
        scratch_shapes=[
            pltpu.VMEM((ROWS, D), BF16),
            pltpu.VMEM((8 * SUBS, SUB, D), BF16),
            pltpu.VMEM((8 * SUBS, SUB, D), BF16),
            pltpu.VMEM((64, 32, 256), BF16),
            pltpu.VMEM((64, 2, 16, 1024), BF16),
            pltpu.VMEM((64, 32, 1152), BF16),
            pltpu.VMEM((2, 16, 128), BF16),
            pltpu.VMEM((1040, 128), F32),
            pltpu.VMEM((1024, 128), F32),
            pltpu.VMEM((8 * SEG, 128), F32),
            pltpu.VMEM((8 * SEG, 128), F32),
            pltpu.VMEM((8 * SEG, 128), F32),
            pltpu.VMEM((8 * SEG, 128), F32),
            pltpu.VMEM((128, 512), BF16),
            pltpu.VMEM((2, 128), F32),
            pltpu.VMEM((16, 128), F32),
            pltpu.VMEM((8, 128, 128), BF16),
            pltpu.VMEM((8, 128, 128), BF16),
            pltpu.VMEM((ROWS, D), F32),
            pltpu.VMEM((ROWS, D), BF16),
            pltpu.VMEM((2 * ROWS, 768), F32),
            pltpu.VMEM((2 * ROWS, 384), BF16),
            pltpu.VMEM((4, ROWS, D), F32),
            pltpu.VMEM((4, ROWS, D), BF16),
            pltpu.VMEM((4, ROWS, D), BF16),
            pltpu.VMEM((3, SUBS, SUB, D), BF16),
            pltpu.VMEM((3, SUBS, SUB, D), BF16),
            dma((8,)),
            dma((64,)),
            dma((64,)),
            dma((64,)),
            dma((3,)),
            dma((8,)),
            dma,
            dma((4,)),
            dma,
            dma((8 * SUBS,)),
            dma((8 * SUBS,)),
            dma((2,)),
            dma((8,)),
            dma,
            dma((4,)),
            dma,
            dma((3, SUBS)),
            dma,
        ],
        compiler_params=pltpu.CompilerParams(
            collective_id=0, has_side_effects=True, vmem_limit_bytes=60 * 1024 * 1024
        ),
    )(
        tokens,
        *gains,
        w_branch,
        w_gelu,
        conv_weight,
        w_rec,
        w_inp,
        decay,
        out_weight_t.reshape(2, 16, 128),
        w_gate,
        w_up,
        down_weight_t,
    )


def solution(mesh):
    return jax.shard_map(
        per_device,
        mesh=mesh,
        in_specs=(
            P(("fs", "tp"), None),
            P(),
            P(),
            P(),
            P(),
            P("fs", "tp"),
            P("fs", "tp"),
            P(None, "tp"),
            P(None, "tp", None, None),
            P(None, "tp", None, None),
            P(None, "tp"),
            P("fs", "tp"),
            P("fs", "tp"),
            P("fs", "tp"),
            P("fs", "tp"),
        ),
        out_specs=P(("fs", "tp"), None),
        check_vma=False,
    )
```

time: 374 us -> 114 us (0.30)
  waiting for transfers between devices: 257 us -> 0 us
  Pallas kernels: 0 us -> 112 us
  local copies, waits for them, and re-layouts: 39.3 us -> 1.88 us
  matrix products: 27.3 us -> 0 us
  other arithmetic: 23.8 us -> 0 us
  between operations: 15 us -> 0.01 us
  blocking collectives: 9.49 us -> 0 us
    all_gather x5 -> x0, waiting for transfers between devices: 215 us -> none  [the longest x2 138 us: in_one_piece(): lax.all_gather(both, axis, axis=dim, tiled=True)]
    pallas_call x0 -> x1, Pallas kernels: none -> 112 us  [per_device(): pl.pallas_call(layer, out_shape=jax.ShapeDtypeStruct((ROWS, D), BF16), in...]
    reduce_scatter x1 -> x0, waiting for transfers between devices: 41.1 us -> none  [summed_rows(): lax.psum_scatter(lax.dot_general(hidden, weight_t, (((1,), (1,)), ((), ()...]
    slice x123 -> x0, local copies, waits for them, and re-layouts: 34.2 us -> none  [the longest x122 32.3 us: recurrence(): unused_decay, states = lax.associative_scan(combine, (retain, feed), axis=0)]
    dot_general x9 -> x0, matrix products: 27.3 us -> none  [the longest x1 9.7 us: summed_rows(): lax.dot_general(hidden, weight_t, (((1,), (1,)), ((), ())), preferred_ele...]
    all_to_all x1 -> x0, blocking collectives: 9.49 us -> none  [per_device(): lax.all_to_all(mixer_hidden, 'tp', split_axis=0, concat_axis=1, tiled=True)]
    concatenate x20 -> x0, other arithmetic: 7.4 us -> none  [the longest x18 4.66 us: recurrence(): unused_decay, states = lax.associative_scan(combine, (retain, feed), axis=0)]
    convert_element_type x5 -> x0, other arithmetic: 6.04 us -> none  [the longest x1 2.09 us: per_device(): return (middle + normed(ffn_sum, post_ffn_gain)).astype(jnp.bfloat16)]
  transfers between devices with their start and end apart: 6 -> 0, of which waited for: 5 -> 0; matrix products, arithmetic and copies ran while one was open for 19% -> 0% of each run, Pallas kernels for 0% -> 0%
where the time goes in v1:
time: 114 us; the launch traced here: 113 us
  Pallas kernels  112 us (98%)
  local copies, waits for them, and re-layouts  1.88 us (2%)
    pallas_call x1, Pallas kernels, per_device(): pl.pallas_call(layer, out_shape=jax.ShapeDtypeStruct((ROWS, D), BF16), in...  112 us

profile of v1, /device:TPU:1, one launch (start us, length us, event | category | flops | bytes accessed | tf_op | source)
XLA Modules:
  0.0 113.5 jit_solution(18407279045788397213)
XLA Ops:
  0.0 111.6 %shard_map.145 = bf16[128,2048]{1,0:T(8,128)(2,1)} custom-call(bf16[128,2048]{1,0:T(8,128)(2,1)} %tokens.1, f32[1,2048]{1,0:T(1,128)} %bitcast.5, f32[1,2048]{1,0:T(1,128)} %bitcast.6, f32[1,2048]{1,0:T(1,128)} %bitcast.7, f32[1,2048]{1,0:T(1,128)} %bitcast.8, bf16[32,128]{1,0:T(8,128)(2,1)} %w_branch.1, bf16[32,128]{1,0:T(8,128)(2,1)} %w_gelu.1, ...), custom_call_target="tpu_custom_call" | custom-call | tf_op jit(solution)/shard_map/pallas_call | solution.py:582
  111.6 1.9 %copy.17 = bf16[128,2048]{1,0:T(8,128)(2,1)} copy(bf16[128,2048]{1,0:T(8,128)(2,1)} %shard_map.145) | data formatting | bytes 1048576

commit v2 on v1

--- a/solution.py
+++ b/solution.py
@@ -33,7 +33,7 @@
 
 
 def sigmoid(v):
-    return 1.0 / (1.0 + jnp.exp(-v))
+    return 0.5 + 0.5 * jnp.tanh(0.5 * v)
 
 
 def gelu(v):
@@ -50,21 +50,29 @@
 
 def layer(
     tokens,
-    pre_mix,
-    post_mix,
-    pre_ffn,
-    post_ffn,
+    pre_mix_hbm,
+    post_mix_hbm,
+    pre_ffn_hbm,
+    post_ffn_hbm,
     w_branch,
     w_gelu,
-    conv_weight,
-    w_rec,
-    w_inp,
-    decay,
+    conv_hbm,
+    w_rec_hbm,
+    w_inp_hbm,
+    decay_hbm,
     out_w,
     w_gate,
     w_up,
     w_down,
     out,
+    pre_mix,
+    post_mix,
+    pre_ffn,
+    post_ffn,
+    conv_weight,
+    w_rec,
+    w_inp,
+    decay,
     tok,
     n1,
     n2,
@@ -92,6 +100,7 @@
     got,
     sums,
     land,
+    final_rows,
     load_sem,
     a_recv,
     o_recv,
@@ -101,8 +110,7 @@
     pre_send,
     swap_recv,
     swap_send,
-    n1_recv,
-    n2_recv,
+    n_recv,
     n_send,
     mix_recv,
     mix_send,
@@ -144,6 +152,14 @@
         (w_gate, f_all.at[f, :, pl.ds(0, 384)]),
         (w_up, f_all.at[f, :, pl.ds(384, 384)]),
         (w_down, f_all.at[f, :, pl.ds(768, 384)]),
+        (pre_mix_hbm, pre_mix),
+        (conv_hbm, conv_weight),
+        (w_rec_hbm, w_rec),
+        (w_inp_hbm, w_inp),
+        (decay_hbm, decay),
+        (post_mix_hbm, post_mix),
+        (pre_ffn_hbm, pre_ffn),
+        (post_ffn_hbm, post_ffn),
     ]
     loads = [pltpu.make_async_copy(s, d, load_sem.at[i]) for i, (s, d) in enumerate(loads)]
     for copy in loads:
@@ -201,6 +217,40 @@
                 self.pass_on(slot, -1)
 
             loop(4, body)
+
+        def spread_near(self):
+            for e in (1, -1, 2, -2):
+                there = place(rem(p + e + RING, RING), q)
+                remote(self.piece(f), self.piece(f), self.send, self.recv.at[f], fs=there).start()
+
+        def relay(self, slot, e):
+            there = place(rem(p + e + RING, RING), q)
+            remote(
+                self.piece(slot), self.piece(slot), self.send, self.recv.at[slot], fs=there
+            ).start()
+
+        def near(self):
+            for j, off in enumerate((0, 1, -1, 2, -2)):
+                slot = place(rem(p + off + RING, RING), q)
+                if j > 0:
+                    self.arrive(slot)
+                if j > 2:
+                    way = 1 if off < 0 else -1
+                    self.relay(slot, way)
+
+                    @pl.when(rem(p, 2) == (0 if off < 0 else 1))
+                    def _():
+                        self.relay(slot, 2 * way)
+
+                self.pass_on(slot, 1)
+                self.pass_on(slot, -1)
+
+        def late(self):
+            for off in (3, -3, 4):
+                slot = place(rem(p + off + RING, RING), q)
+                self.arrive(slot)
+                self.pass_on(slot, 1)
+                self.pass_on(slot, -1)
 
         def hop(self, far, half):
             def body(i):
@@ -239,7 +289,7 @@
         remote(
             o_own.at[half], o_all.at[f, half, :, own_lanes], pre_send, pre_recv.at[t], tp=other
         ).start()
-    own_out = pltpu.make_async_copy(o_own.at[c], o_all.at[f, c, :, own_lanes], load_sem.at[7])
+    own_out = pltpu.make_async_copy(o_own.at[c], o_all.at[f, c, :, own_lanes], load_sem.at[15])
     own_out.start()
 
     class Rows:
@@ -285,10 +335,11 @@
             rows = self.ref[pl.ds(tp * SUBS, SUBS)]
             return rows.reshape(ROWS, D)
 
-    r1 = Rows(n1, n1_recv, n_send.at[0])
-    r2 = Rows(n2, n2_recv, n_send.at[1])
+    r1 = Rows(n1, n_recv, n_send.at[0])
+    r2 = Rows(n2, n_recv, n_send.at[1])
 
     loads[3].wait()
+    loads[7].wait()
 
     def norm_in(k):
         for h in range(SUB // 16):
@@ -298,8 +349,8 @@
 
     loop(SUBS, norm_in)
 
-    ga.first(0)
-    ga.first(1)
+    for i in range(8, 12):
+        loads[i].wait()
     for d in range(2):
         gates[:, pl.ds(256 * d, 128)] = w_rec[d, 0]
         gates[:, pl.ds(256 * d + 128, 128)] = w_inp[d, 0]
@@ -308,32 +359,38 @@
     branch[pl.ds(0, 8), :] = jnp.zeros((8, 128), F32)
     branch[pl.ds(1032, 8), :] = jnp.zeros((8, 128), F32)
 
+    ga.first(0)
+    ga.first(1)
     own_out.wait()
     for e in range(1, 8):
         other = rem(t + e, 8)
         lanes = pl.ds(pl.multiple_of(other * 128, 128), 128)
         hold(o_all.at[f, c, :, lanes], pre_recv.at[other])
-    ga.hop(1, 0)
-    go.spread()
-    ga.hop(1, 1)
+    go.spread_near()
     r1.behind(0)
     r1.ahead(0)
-    ga.hop(2, 0)
-    ga.hop(2, 1)
+    ga.hop(1, 0)
+    ga.hop(1, 1)
     r1.behind(1)
     r1.ahead(1)
-    go.first(0)
-    ga.hop(3, 0)
-    go.first(1)
+    ga.hop(2, 0)
+    go.near()
     r1.behind(2)
     r1.ahead(2)
-    loads[4].wait()
-    loads[5].wait()
-    loads[6].wait()
-    gf.spread()
-    ga.finish()
+    ga.hop(2, 1)
     r1.behind(3)
     r1.ahead(3)
+    for i in (4, 5, 6, 12, 13, 14):
+        loads[i].wait()
+    ga.hop(3, 0)
+    go.late()
+    gf.spread_near()
+    go.hop(1, 0)
+    for k in range(2):
+        r1.far(k)
+    ga.finish()
+    for k in range(2, SUBS):
+        r1.far(k)
 
     def project(chip_at):
         r1.paired(chip_at)
@@ -345,13 +402,10 @@
         gel[pl.ds(pl.multiple_of(at, 8), 2 * ROWS), :] = both[:, 128:]
 
     project(x)
-    go.hop(1, 0)
     project(chip(turn))
     go.hop(1, 1)
     project(chip(-turn))
     go.hop(2, 0)
-    for k in range(SUBS):
-        r1.far(k)
     project(chip(2))
 
     taps = conv_weight[...].astype(F32)
@@ -378,8 +432,10 @@
             ret[at, :] = retain
             fee[at, :] = jnp.sqrt(lost) * inflow * wide
 
-    loop(8, gate)
+    loop(4, gate)
     go.hop(2, 1)
+    loop(4, lambda s: gate(s + 4))
+    gf.near()
 
     one, zero = jnp.ones((8, 128), F32), jnp.zeros((8, 128), F32)
 
@@ -428,8 +484,7 @@
 
     loop(8, mix)
     go.hop(3, 0)
-    gf.first(0)
-    gf.first(1)
+    gf.late()
     go.finish()
 
     def swap(part):
@@ -437,10 +492,10 @@
         remote(rows, rows, swap_send, swap_recv.at[part], tp=partner).start()
 
     loop(4, swap)
+    gf.hop(1, 0)
     for e in range(1, 8):
         other = rem(t + e, 8)
         hold(hidden.at[other], mix_recv.at[other])
-    gf.hop(1, 0)
 
     wide_hidden = jnp.concatenate([hidden[i] for i in range(8)], axis=1)
 
@@ -467,20 +522,24 @@
     loop(SUBS, norm_mid)
     gf.hop(1, 1)
     gf.hop(2, 0)
-    for k in range(SUBS):
-        r2.behind(k)
-        r2.ahead(k)
+    r2.behind(0)
+    r2.ahead(0)
     gf.hop(2, 1)
+    r2.behind(1)
+    r2.ahead(1)
+    r2.behind(2)
+    r2.ahead(2)
     gf.hop(3, 0)
-    for k in range(SUBS):
-        r2.far(k)
+    r2.behind(3)
+    r2.ahead(3)
     gf.finish()
 
-    def feed_forward(i):
-        away = jnp.where(i == 0, 2, jnp.where(i == 1, -turn, jnp.where(i == 2, turn, 0)))
-        there = chip(away)
-        r2.paired(there)
-        rows = jnp.concatenate([r2.block(2 * there + 1 - c), r2.block(2 * there + c)], axis=0)
+    def feed_up(i):
+        away = 2 if i == 0 else 0 if i == 3 else -turn if i == 1 else turn
+        mine = chip(away)
+        theirs = chip(-away)
+        r2.paired(theirs)
+        rows = jnp.concatenate([r2.block(2 * theirs + 1 - c), r2.block(2 * mine + c)], axis=0)
         for n in range(3):
             gu[:, pl.ds(256 * n, 256)] = jnp.dot(
                 rows, f_all[:, :, pl.ds(256 * n, 256)].reshape(D, 256), preferred_element_type=F32
@@ -490,6 +549,7 @@
             g = gu[at, pl.ds(0, 384)]
             hid[at, :] = (g * sigmoid(g) * gu[at, pl.ds(384, 384)]).astype(BF16)
 
+    def feed_down(i):
         def down(n):
             weight = f_all[pl.ds(16 * n, 16), :, pl.ds(768, 384)].reshape(512, 384)
             part = lax.dot_general(hid[...], weight, NT, preferred_element_type=F32)
@@ -498,12 +558,7 @@
             keep[i, :, lanes] = part[ROWS:]
 
         loop(4, down)
-        other = jnp.where(i == 1, 2, jnp.where(i == 2, 1, i))
-        remote(give.at[i], got.at[other], pair_send, pair_recv.at[other], tp=partner).start()
-
-        @pl.when(i == 1)
-        def _():
-            pass_sum(0)
+        remote(give.at[i], got.at[i], pair_send, pair_recv.at[i], tp=partner).start()
 
     def pass_sum(o):
         target = 2 * chip(-turn if o == 1 else turn) + c
@@ -525,8 +580,18 @@
 
         loop(SUBS, add)
 
-    loop(4, feed_forward)
+    feed_up(1)
+    feed_down(1)
+    for k in range(SUBS):
+        r2.far(k)
+    feed_up(2)
     pass_sum(1)
+    feed_down(2)
+    feed_up(0)
+    feed_down(0)
+    feed_up(3)
+    pass_sum(0)
+    feed_down(3)
     pass_sum(2)
     hold(got.at[3], pair_recv.at[3])
 
@@ -540,10 +605,14 @@
             total = total + land[1, k, inner, :].astype(F32)
             total = total + land[2, k, inner, :].astype(F32)
             final = res[at, :].astype(F32) + normed(total, post_ffn[...])
-            out[at, :] = final.astype(BF16)
+            final_rows[at, :] = final.astype(BF16)
+        rows = pl.ds(pl.multiple_of(k * SUB, SUB), SUB)
+        pltpu.make_async_copy(final_rows.at[rows], out.at[rows], load_sem.at[k]).start()
 
     loop(SUBS, last)
 
+    for k in range(SUBS):
+        hold(final_rows.at[pl.ds(0, SUB)], load_sem.at[k])
     hold(a_all.at[pl.ds(0, 63)], ring_send.at[0])
     hold(o_all.at[pl.ds(0, 63), 0], ring_send.at[1])
     hold(f_all.at[pl.ds(0, 63)], ring_send.at[2])
@@ -576,15 +645,22 @@
     gains = [
         g.reshape(1, D) for g in (pre_mix_gain, post_mix_gain, pre_ffn_gain, post_ffn_gain)
     ]
-    vmem = pl.BlockSpec(memory_space=pltpu.VMEM)
-    far = pl.BlockSpec(memory_space=pl.ANY)
+    far = pl.BlockSpec(memory_space=pltpu.HBM)
     dma = pltpu.SemaphoreType.DMA
     return pl.pallas_call(
         layer,
         out_shape=jax.ShapeDtypeStruct((ROWS, D), BF16),
-        in_specs=[far] + [vmem] * 4 + [far, far] + [vmem] * 4 + [far] * 4,
-        out_specs=vmem,
+        in_specs=[far] * 15,
+        out_specs=far,
         scratch_shapes=[
+            pltpu.VMEM((1, D), F32),
+            pltpu.VMEM((1, D), F32),
+            pltpu.VMEM((1, D), F32),
+            pltpu.VMEM((1, D), F32),
+            pltpu.VMEM((4, 128), BF16),
+            pltpu.VMEM((2, 1, 128, 128), BF16),
+            pltpu.VMEM((2, 1, 128, 128), BF16),
+            pltpu.VMEM((2, 128), F32),
             pltpu.VMEM((ROWS, D), BF16),
             pltpu.VMEM((8 * SUBS, SUB, D), BF16),
             pltpu.VMEM((8 * SUBS, SUB, D), BF16),
@@ -612,7 +688,8 @@
             pltpu.VMEM((4, ROWS, D), BF16),
             pltpu.VMEM((3, SUBS, SUB, D), BF16),
             pltpu.VMEM((3, SUBS, SUB, D), BF16),
-            dma((8,)),
+            pltpu.VMEM((ROWS, D), BF16),
+            dma((16,)),
             dma((64,)),
             dma((64,)),
             dma((64,)),
@@ -621,7 +698,6 @@
             dma,
             dma((4,)),
             dma,
-            dma((8 * SUBS,)),
             dma((8 * SUBS,)),
             dma((2,)),
             dma((8,)),

time: 114 us -> 103 us (0.904)
  Pallas kernels: 112 us -> 101 us
    pallas_call x1, Pallas kernels: 112 us -> 101 us  [per_device(): pl.pallas_call(layer, out_shape=jax.ShapeDtypeStruct((ROWS, D), BF16), in...]
where the time goes in v2:
time: 103 us
  Pallas kernels  101 us (98%)
  local copies, waits for them, and re-layouts  1.88 us (2%)
    pallas_call x1, Pallas kernels, per_device(): pl.pallas_call(layer, out_shape=jax.ShapeDtypeStruct((ROWS, D), BF16), in...  101 us

profile of v2, /device:TPU:1, one launch (start us, length us, event | category | flops | bytes accessed | tf_op | source)
XLA Modules:
  0.0 103.3 jit_solution(16925751620864529741)
XLA Ops:
  0.0 101.5 %shard_map.145 = bf16[128,2048]{1,0:T(8,128)(2,1)} custom-call(bf16[128,2048]{1,0:T(8,128)(2,1)} %tokens.1, f32[1,2048]{1,0:T(1,128)} %bitcast.5, f32[1,2048]{1,0:T(1,128)} %bitcast.6, f32[1,2048]{1,0:T(1,128)} %bitcast.7, f32[1,2048]{1,0:T(1,128)} %bitcast.8, bf16[32,128]{1,0:T(8,128)(2,1)} %w_branch.1, bf16[32,128]{1,0:T(8,128)(2,1)} %w_gelu.1, ...), custom_call_target="tpu_custom_call" | custom-call | tf_op jit(solution)/shard_map/pallas_call | solution.py:650
  101.5 1.9 %copy.17 = bf16[128,2048]{1,0:T(8,128)(2,1)} copy(bf16[128,2048]{1,0:T(8,128)(2,1)} %shard_map.145) | data formatting | bytes 1048576

commit v3 on v2

--- a/solution.py
+++ b/solution.py
@@ -16,6 +16,7 @@
 SUBS = ROWS // SUB
 D = 2048
 SEG = 136
+WIDE = (2, -2, 1, -1)
 NT = (((1,), (1,)), ((), ()))
 
 
@@ -100,6 +101,7 @@
     got,
     sums,
     land,
+    power,
     final_rows,
     load_sem,
     a_recv,
@@ -172,15 +174,36 @@
 
     for e in range(1, RING):
         greet(place(rem(p + e, RING), q), t)
-    for e in (1, RING - 1):
+    for e in (1, 2, RING - 2, RING - 1):
         greet(place(p, rem(q + e, RING)), t)
     for e in range(1, 8):
         greet(f, rem(t + e, 8))
-    pl.semaphore_wait(barrier, 16)
+    loads[3].wait()
+    loads[7].wait()
+
+    def norm_in(k):
+        for h in range(SUB // 16):
+            rows = tok[pl.ds(pl.multiple_of(k * SUB + 16 * h, 16), 16), :].astype(F32)
+            n1[t * SUBS + k, pl.ds(16 * h, 16), :] = normed(rows, pre_mix[...]).astype(BF16)
+
+    loop(SUBS, norm_in)
+
+    for i in range(8, 12):
+        loads[i].wait()
+    for d in range(2):
+        gates[:, pl.ds(256 * d, 128)] = w_rec[d, 0]
+        gates[:, pl.ds(256 * d + 128, 128)] = w_inp[d, 0]
+    low = -decay[...]
+    scale[...] = -8.0 * (jnp.maximum(low, 0.0) + jnp.log1p(jnp.exp(-jnp.abs(low))))
+    branch[pl.ds(0, 8), :] = jnp.zeros((8, 128), F32)
+    branch[pl.ds(1032, 8), :] = jnp.zeros((8, 128), F32)
+
+    pl.semaphore_wait(barrier, 18)
 
     class Gather:
-        def __init__(self, piece, recv, send):
+        def __init__(self, piece, recv, send, share=None):
             self.piece, self.recv, self.send = piece, recv, send
+            self.share = share or (lambda slot: None)
 
         def spread(self):
             def body(e):
@@ -203,6 +226,7 @@
 
         def arrive(self, slot):
             hold(self.piece(slot), self.recv.at[slot])
+            self.share(slot)
 
         def first(self, half):
             def body(i):
@@ -217,6 +241,41 @@
                 self.pass_on(slot, -1)
 
             loop(4, body)
+
+        def first_wide(self, half):
+            def body(i):
+                j = i + 4 * half
+                slot = self.slot(j, 0)
+
+                @pl.when(j > 0)
+                def _():
+                    self.arrive(slot)
+
+                for way in (2, -2, 1, -1):
+                    self.pass_on(slot, way)
+
+            loop(4, body)
+
+        def relay_wide(self, low, count):
+            def body(i):
+                j = i + low
+                for way in (1, -1):
+                    slot = self.slot(j, -2 * way)
+                    self.arrive(slot)
+                    self.pass_on(slot, way)
+
+                    @pl.when(rem(j, 2) == (0 if way > 0 else 1))
+                    def _():
+                        self.pass_on(slot, 2 * way)
+
+            loop(count, body)
+
+        def finish_wide(self):
+            def body(j):
+                for away in (1, -1, 3, -3, 4):
+                    self.arrive(self.slot(j, away))
+
+            loop(8, body)
 
         def spread_near(self):
             for e in (1, -1, 2, -2):
@@ -229,11 +288,13 @@
                 self.piece(slot), self.piece(slot), self.send, self.recv.at[slot], fs=there
             ).start()
 
-        def near(self):
+        def near(self, ways=(1, -1)):
             for j, off in enumerate((0, 1, -1, 2, -2)):
                 slot = place(rem(p + off + RING, RING), q)
                 if j > 0:
                     self.arrive(slot)
+                else:
+                    self.share(slot)
                 if j > 2:
                     way = 1 if off < 0 else -1
                     self.relay(slot, way)
@@ -242,15 +303,15 @@
                     def _():
                         self.relay(slot, 2 * way)
 
-                self.pass_on(slot, 1)
-                self.pass_on(slot, -1)
-
-        def late(self):
+                for way in ways:
+                    self.pass_on(slot, way)
+
+        def late(self, ways=(1, -1)):
             for off in (3, -3, 4):
                 slot = place(rem(p + off + RING, RING), q)
                 self.arrive(slot)
-                self.pass_on(slot, 1)
-                self.pass_on(slot, -1)
+                for way in ways:
+                    self.pass_on(slot, way)
 
         def hop(self, far, half):
             def body(i):
@@ -274,7 +335,11 @@
             loop(4, body)
 
     ga = Gather(lambda s: a_all.at[s], a_recv, ring_send.at[0])
-    go = Gather(lambda s: o_all.at[s, c], o_recv, ring_send.at[1])
+    def share(slot):
+        rows = o_all.at[slot, c]
+        remote(rows, rows, swap_send, swap_recv, tp=partner).start()
+
+    go = Gather(lambda s: o_all.at[s, c], o_recv, ring_send.at[1], share)
     gf = Gather(lambda s: f_all.at[s], f_recv, ring_send.at[2])
 
     loads[0].wait()
@@ -338,29 +403,13 @@
     r1 = Rows(n1, n_recv, n_send.at[0])
     r2 = Rows(n2, n_recv, n_send.at[1])
 
-    loads[3].wait()
-    loads[7].wait()
-
-    def norm_in(k):
-        for h in range(SUB // 16):
-            rows = tok[pl.ds(pl.multiple_of(k * SUB + 16 * h, 16), 16), :].astype(F32)
-            n1[t * SUBS + k, pl.ds(16 * h, 16), :] = normed(rows, pre_mix[...]).astype(BF16)
-        r1.own(k)
-
-    loop(SUBS, norm_in)
-
-    for i in range(8, 12):
+    loop(SUBS, r1.own)
+
+    for i in (4, 5, 6, 12, 13, 14):
         loads[i].wait()
-    for d in range(2):
-        gates[:, pl.ds(256 * d, 128)] = w_rec[d, 0]
-        gates[:, pl.ds(256 * d + 128, 128)] = w_inp[d, 0]
-    low = -decay[...]
-    scale[...] = -8.0 * (jnp.maximum(low, 0.0) + jnp.log1p(jnp.exp(-jnp.abs(low))))
-    branch[pl.ds(0, 8), :] = jnp.zeros((8, 128), F32)
-    branch[pl.ds(1032, 8), :] = jnp.zeros((8, 128), F32)
-
-    ga.first(0)
-    ga.first(1)
+    gf.spread_near()
+    ga.first_wide(0)
+    ga.first_wide(1)
     own_out.wait()
     for e in range(1, 8):
         other = rem(t + e, 8)
@@ -369,28 +418,19 @@
     go.spread_near()
     r1.behind(0)
     r1.ahead(0)
-    ga.hop(1, 0)
-    ga.hop(1, 1)
+    ga.relay_wide(0, 4)
+    ga.relay_wide(4, 4)
     r1.behind(1)
     r1.ahead(1)
-    ga.hop(2, 0)
     go.near()
+    gf.near()
     r1.behind(2)
     r1.ahead(2)
-    ga.hop(2, 1)
     r1.behind(3)
     r1.ahead(3)
-    for i in (4, 5, 6, 12, 13, 14):
-        loads[i].wait()
-    ga.hop(3, 0)
+    ga.finish_wide()
     go.late()
-    gf.spread_near()
     go.hop(1, 0)
-    for k in range(2):
-        r1.far(k)
-    ga.finish()
-    for k in range(2, SUBS):
-        r1.far(k)
 
     def project(chip_at):
         r1.paired(chip_at)
@@ -401,12 +441,16 @@
         branch[pl.ds(pl.multiple_of(at + 8, 8), 2 * ROWS), :] = both[:, :128]
         gel[pl.ds(pl.multiple_of(at, 8), 2 * ROWS), :] = both[:, 128:]
 
+    r1.far(0)
+    r1.far(1)
     project(x)
+    r1.far(2)
     project(chip(turn))
+    r1.far(3)
+    project(chip(-turn))
     go.hop(1, 1)
-    project(chip(-turn))
+    project(chip(2))
     go.hop(2, 0)
-    project(chip(2))
 
     taps = conv_weight[...].astype(F32)
 
@@ -435,7 +479,6 @@
     loop(4, gate)
     go.hop(2, 1)
     loop(4, lambda s: gate(s + 4))
-    gf.near()
 
     one, zero = jnp.ones((8, 128), F32), jnp.zeros((8, 128), F32)
 
@@ -467,18 +510,20 @@
         state = a1[s : s + 1] * state + h1[s : s + 1]
 
     def mix(e):
-        s = rem(t + e, 8)
+        m = lax.div(e, jnp.int32(2))
+        away = jnp.where(m == 3, 0, jnp.where(m == 2, 3, 2 - m))
+        s = 2 * chip(away) + rem(c + 1 + e, 2)
         at = pl.ds(pl.multiple_of(s * SEG, 8), 128)
         state = fee0[at, :] + ret0[at, :] * carry_in[pl.ds(s, 1), :]
         state = state + (fee1[at, :] + ret1[at, :] * carry_in[pl.ds(8 + s, 1), :])
         value = gelu(gel[pl.ds(pl.multiple_of(s * 128, 8), 128), :]) * state
         mixed[s] = value.astype(BF16)
 
-        @pl.when(e > 0)
+        @pl.when(e < 7)
         def _():
             remote(mixed.at[s], hidden.at[t], mix_send, mix_recv.at[t], tp=s).start()
 
-        @pl.when(e == 0)
+        @pl.when(e == 7)
         def _():
             hidden[s] = value.astype(BF16)
 
@@ -486,12 +531,6 @@
     go.hop(3, 0)
     gf.late()
     go.finish()
-
-    def swap(part):
-        rows = o_all.at[pl.ds(16 * part, 16), c]
-        remote(rows, rows, swap_send, swap_recv.at[part], tp=partner).start()
-
-    loop(4, swap)
     gf.hop(1, 0)
     for e in range(1, 8):
         other = rem(t + e, 8)
@@ -499,8 +538,9 @@
 
     wide_hidden = jnp.concatenate([hidden[i] for i in range(8)], axis=1)
 
+    hold(o_all.at[:, 1 - c], swap_recv)
+
     def project_out(part):
-        hold(o_all.at[pl.ds(16 * part, 16), 1 - c], swap_recv.at[part])
         weight = o_all[pl.ds(16 * part, 16)].reshape(512, 1024)
         msum[:, pl.ds(pl.multiple_of(part * 512, 128), 512)] = lax.dot_general(
             wide_hidden, weight, NT, preferred_element_type=F32
@@ -553,59 +593,77 @@
         def down(n):
             weight = f_all[pl.ds(16 * n, 16), :, pl.ds(768, 384)].reshape(512, 384)
             part = lax.dot_general(hid[...], weight, NT, preferred_element_type=F32)
-            lanes = pl.ds(pl.multiple_of(512 * n, 128), 512)
-            give[i, :, lanes] = part[:ROWS].astype(BF16)
-            keep[i, :, lanes] = part[ROWS:]
+            give[i, n] = part[:ROWS].astype(BF16)
+            keep[i, n] = part[ROWS:]
+            remote(
+                give.at[i, n], got.at[i, n], pair_send, pair_recv.at[i, n], tp=partner
+            ).start()
 
         loop(4, down)
-        remote(give.at[i], got.at[i], pair_send, pair_recv.at[i], tp=partner).start()
-
-    def pass_sum(o):
+
+    def pass_sum(o, low, count):
         target = 2 * chip(-turn if o == 1 else turn) + c
-        hold(got.at[o], pair_recv.at[o])
-
-        def add(k):
+
+        def add(m):
+            n = m + low
+            hold(got.at[o, n], pair_recv.at[o, n])
             if o == 2:
-                hold(land.at[0, k], land_recv.at[0, k])
-            for h in range(SUB // 16):
-                at = pl.ds(pl.multiple_of(k * SUB + 16 * h, 16), 16)
-                inner = pl.ds(16 * h, 16)
-                total = keep[o, at, :] + got[o, at, :].astype(F32)
+                hold(land.at[0, n], land_recv.at[0, n])
+            for h in range(ROWS // SUB):
+                at = pl.ds(SUB * h, SUB)
+                total = keep[o, n, at, :] + got[o, n, at, :].astype(F32)
                 if o == 2:
-                    total = total + land[0, k, inner, :].astype(F32)
-                sums[o, k, inner, :] = total.astype(BF16)
+                    total = total + land[0, n, at, :].astype(F32)
+                sums[o, n, at, :] = total.astype(BF16)
             remote(
-                sums.at[o, k], land.at[o, k], land_send, land_recv.at[o, k], tp=target
+                sums.at[o, n], land.at[o, n], land_send, land_recv.at[o, n], tp=target
             ).start()
 
-        loop(SUBS, add)
+        loop(count, add)
 
     feed_up(1)
     feed_down(1)
     for k in range(SUBS):
         r2.far(k)
+    pass_sum(1, 0, 2)
     feed_up(2)
-    pass_sum(1)
+    pass_sum(1, 2, 2)
     feed_down(2)
     feed_up(0)
     feed_down(0)
+    pass_sum(0, 0, 2)
     feed_up(3)
-    pass_sum(0)
+    pass_sum(0, 2, 2)
     feed_down(3)
-    pass_sum(2)
-    hold(got.at[3], pair_recv.at[3])
+    pass_sum(2, 0, 4)
+
+    power[...] = jnp.zeros_like(power)
+
+    def own_sum(n):
+        hold(got.at[3, n], pair_recv.at[3, n])
+        hold(land.at[1, n], land_recv.at[1, n])
+        hold(land.at[2, n], land_recv.at[2, n])
+        for h in range(ROWS // SUB):
+            at = pl.ds(SUB * h, SUB)
+            total = keep[3, n, at, :] + got[3, n, at, :].astype(F32)
+            total = total + land[1, n, at, :].astype(F32)
+            total = total + land[2, n, at, :].astype(F32)
+            keep[3, n, at, :] = total
+            square = total * total
+            square = square[:, :256] + square[:, 256:]
+            power[at, :] += square[:, :128] + square[:, 128:]
+
+    loop(4, own_sum)
 
     def last(k):
-        hold(land.at[1, k], land_recv.at[1, k])
-        hold(land.at[2, k], land_recv.at[2, k])
         for h in range(SUB // 16):
             at = pl.ds(pl.multiple_of(k * SUB + 16 * h, 16), 16)
-            inner = pl.ds(16 * h, 16)
-            total = keep[3, at, :] + got[3, at, :].astype(F32)
-            total = total + land[1, k, inner, :].astype(F32)
-            total = total + land[2, k, inner, :].astype(F32)
-            final = res[at, :].astype(F32) + normed(total, post_ffn[...])
-            final_rows[at, :] = final.astype(BF16)
+            mean = jnp.sum(power[at, :], axis=-1, keepdims=True) * (1.0 / D)
+            factor = lax.rsqrt(mean + EPS)
+            for n in range(4):
+                lanes = pl.ds(512 * n, 512)
+                value = keep[3, n, at, :] * factor * post_ffn[:, lanes]
+                final_rows[at, lanes] = (res[at, lanes].astype(F32) + value).astype(BF16)
         rows = pl.ds(pl.multiple_of(k * SUB, SUB), SUB)
         pltpu.make_async_copy(final_rows.at[rows], out.at[rows], load_sem.at[k]).start()
 
@@ -683,11 +741,12 @@
             pltpu.VMEM((ROWS, D), BF16),
             pltpu.VMEM((2 * ROWS, 768), F32),
             pltpu.VMEM((2 * ROWS, 384), BF16),
-            pltpu.VMEM((4, ROWS, D), F32),
-            pltpu.VMEM((4, ROWS, D), BF16),
-            pltpu.VMEM((4, ROWS, D), BF16),
-            pltpu.VMEM((3, SUBS, SUB, D), BF16),
-            pltpu.VMEM((3, SUBS, SUB, D), BF16),
+            pltpu.VMEM((4, 4, ROWS, 512), F32),
+            pltpu.VMEM((4, 4, ROWS, 512), BF16),
+            pltpu.VMEM((4, 4, ROWS, 512), BF16),
+            pltpu.VMEM((3, 4, ROWS, 512), BF16),
+            pltpu.VMEM((3, 4, ROWS, 512), BF16),
+            pltpu.VMEM((ROWS, 128), F32),
             pltpu.VMEM((ROWS, D), BF16),
             dma((16,)),
             dma((64,)),
@@ -696,15 +755,15 @@
             dma((3,)),
             dma((8,)),
             dma,
-            dma((4,)),
+            dma,
             dma,
             dma((8 * SUBS,)),
             dma((2,)),
             dma((8,)),
             dma,
-            dma((4,)),
+            dma((4, 4)),
             dma,
-            dma((3, SUBS)),
+            dma((3, 4)),
             dma,
         ],
         compiler_params=pltpu.CompilerParams(

time: 103 us -> 96.6 us (0.938)
  Pallas kernels: 101 us -> 94.5 us
    pallas_call x1, Pallas kernels: 101 us -> 94.5 us  [per_device(): pl.pallas_call(layer, out_shape=jax.ShapeDtypeStruct((ROWS, D), BF16), in...]
where the time goes in v3:
time: 96.6 us; the launch traced here: 96.4 us
  Pallas kernels  94.5 us (98%)
  local copies, waits for them, and re-layouts  1.88 us (2%)
    pallas_call x1, Pallas kernels, per_device(): pl.pallas_call(layer, out_shape=jax.ShapeDtypeStruct((ROWS, D), BF16), in...  94.5 us

profile of v3, /device:TPU:1, one launch (start us, length us, event | category | flops | bytes accessed | tf_op | source)
XLA Modules:
  0.0 96.4 jit_solution(15401420939716417360)
XLA Ops:
  0.0 94.5 %shard_map.145 = bf16[128,2048]{1,0:T(8,128)(2,1)} custom-call(bf16[128,2048]{1,0:T(8,128)(2,1)} %tokens.1, f32[1,2048]{1,0:T(1,128)} %bitcast.5, f32[1,2048]{1,0:T(1,128)} %bitcast.6, f32[1,2048]{1,0:T(1,128)} %bitcast.7, f32[1,2048]{1,0:T(1,128)} %bitcast.8, bf16[32,128]{1,0:T(8,128)(2,1)} %w_branch.1, bf16[32,128]{1,0:T(8,128)(2,1)} %w_gelu.1, ...), custom_call_target="tpu_custom_call" | custom-call | tf_op jit(solution)/shard_map/pallas_call | solution.py:708
  94.5 1.9 %copy.17 = bf16[128,2048]{1,0:T(8,128)(2,1)} copy(bf16[128,2048]{1,0:T(8,128)(2,1)} %shard_map.145) | data formatting | bytes 1048576

commit v4 on v3

--- a/solution.py
+++ b/solution.py
@@ -325,6 +325,14 @@
 
             loop(4, body)
 
+        def hop_last(self, way):
+            def body(j):
+                slot = self.slot(j if way > 0 else j + 4, -3 * way)
+                self.arrive(slot)
+                self.pass_on(slot, way)
+
+            loop(4, body)
+
         def finish(self):
             def body(j):
                 self.arrive(self.slot(j + 4, -3))
@@ -530,8 +538,8 @@
     loop(8, mix)
     go.hop(3, 0)
     gf.late()
+    gf.hop(1, 0)
     go.finish()
-    gf.hop(1, 0)
     for e in range(1, 8):
         other = rem(t + e, 8)
         hold(hidden.at[other], mix_recv.at[other])
@@ -567,9 +575,10 @@
     gf.hop(2, 1)
     r2.behind(1)
     r2.ahead(1)
+    gf.hop_last(1)
     r2.behind(2)
     r2.ahead(2)
-    gf.hop(3, 0)
+    gf.hop_last(-1)
     r2.behind(3)
     r2.ahead(3)
     gf.finish()

time: 96.6 us -> 95.9 us (level)
  no operation moved by 1% of the time
where the time goes in v4:
time: 95.9 us; the launch traced here: 95.7 us
  Pallas kernels  93.9 us (98%)
  local copies, waits for them, and re-layouts  1.88 us (2%)
    pallas_call x1, Pallas kernels, per_device(): pl.pallas_call(layer, out_shape=jax.ShapeDtypeStruct((ROWS, D), BF16), in...  93.9 us

profile of v4, /device:TPU:1, one launch (start us, length us, event | category | flops | bytes accessed | tf_op | source)
XLA Modules:
  0.0 95.7 jit_solution(8368044729953708583)
XLA Ops:
  0.0 93.9 %shard_map.145 = bf16[128,2048]{1,0:T(8,128)(2,1)} custom-call(bf16[128,2048]{1,0:T(8,128)(2,1)} %tokens.1, f32[1,2048]{1,0:T(1,128)} %bitcast.5, f32[1,2048]{1,0:T(1,128)} %bitcast.6, f32[1,2048]{1,0:T(1,128)} %bitcast.7, f32[1,2048]{1,0:T(1,128)} %bitcast.8, bf16[32,128]{1,0:T(8,128)(2,1)} %w_branch.1, bf16[32,128]{1,0:T(8,128)(2,1)} %w_gelu.1, ...), custom_call_target="tpu_custom_call" | custom-call | tf_op jit(solution)/shard_map/pallas_call | solution.py:717
  93.9 1.9 %copy.17 = bf16[128,2048]{1,0:T(8,128)(2,1)} copy(bf16[128,2048]{1,0:T(8,128)(2,1)} %shard_map.145) | data formatting | bytes 1048576
